TPU v7x, 32 devices: a whole 2x2x4 slice. The times are simulated.
32 devices in a mesh: kv: 16 (over z, y, x), tp: 2 (over core).
Axes of the slice: x: 2, y: 2, z: 4, core: 2. Of those that a mesh axis runs over, the one named last changes fastest.
Arguments:
- tokens: bfloat16 [64, 2048], P('tp', 'kv'), may hold values from -60 to 60
- gain_mix: float32 [2048], P('kv'), may hold values from 0.1 to 1.9
- w_query: bfloat16 [2048, 2048], P('kv', 'tp'), may hold values from -0.125 to 0.125
- w_key: bfloat16 [2048, 2048], P('kv', 'tp'), may hold values from -0.125 to 0.125
- w_value: bfloat16 [2048, 2048], P('kv', 'tp'), may hold values from -0.125 to 0.125
- w_igate: bfloat16 [2048, 8], P('kv', 'tp'), may hold values from -0.125 to 0.125
- w_fgate: bfloat16 [2048, 8], P('kv', 'tp'), may hold values from -0.125 to 0.125
- bias_igate: float32 [8], P('tp'), may hold values from -3 to 3
- bias_fgate: float32 [8], P('tp'), may hold values from -3 to 3
- state_mem: float32 [64, 8, 256, 256], P('kv', 'tp'), may hold values from -2 to 2
- state_max: float32 [64, 8], P('kv', 'tp'), may hold values from -60 to 220
- keys_blk: bfloat16 [64, 8, 128, 256], P('kv', 'tp'), may hold values from -6 to 6
- values_blk: bfloat16 [64, 8, 128, 256], P('kv', 'tp'), may hold values from -6 to 6
- igate_blk: float32 [64, 8, 128], P('kv', 'tp'), may hold values from -10 to 220
- fgate_blk: float32 [64, 8, 128], P('kv', 'tp'), may hold values from -3 to 0
- lengths: int32 [64], P('kv'), may hold values from 1 to 127, 2048 in all
- gain_head: float32 [256], replicated, may hold values from 0.1 to 1.9
- w_mixout: bfloat16 [2048, 2048], P('tp', 'kv'), may hold values from -0.25 to 0.25
- gain_mlp: float32 [2048], P('kv'), may hold values from 0.1 to 1.9
- w_up: bfloat16 [2048, 8192], P('kv', 'tp'), may hold values from -0.125 to 0.125
- w_down: bfloat16 [8192, 2048], P('tp', 'kv'), may hold values from -0.0625 to 0.0625
Outputs:
- layer_out: bfloat16 [64, 2048], P('tp', 'kv')
Inputs may be any that keep to these rules, and one draw needn't show every extreme that they name: `lengths`: entries of a sequence's block at or past its length are not live. The largest length is reached in every draw.
All inputs are finite; a program needn't handle non-finite values.
Results may differ from a plain program's by a relative error of at most 0.015.
Values may be sent and summed in bfloat16 or wider, within the bound.
A program may use at most 64 MiB of HBM per device.

v0:
```python
import functools
import jax
import jax.numpy as jnp
from jax import lax
from jax.experimental import pallas as pl
from jax.experimental.pallas import tpu as pltpu
from jax.sharding import PartitionSpec as P

EPS = 1e-06
F32 = jnp.float32
BF16 = jnp.bfloat16
MESH = pl.DeviceIdType.MESH


def ceil_chunks(width):
    return 2 if width % 256 == 0 else 1


def inner_size(count):
    return max(d for d in range(1, count + 1) if count % d == 0 and d * d <= count)


def kernel(
    cfg,
    tokens,
    gain_mix,
    w_query,
    w_key,
    w_value,
    w_igate,
    w_fgate,
    bias_igate,
    bias_fgate,
    state_mem,
    state_max,
    keys_blk,
    values_blk,
    igate_blk,
    fgate_blk,
    lengths,
    gain_head,
    w_mixout,
    gain_mlp,
    w_up,
    w_down,
    out,
    wq_v,
    wk_v,
    wv_v,
    state_v,
    state_hi,
    state_lo,
    keys_v,
    values_v,
    wo_v,
    wu_v,
    wd_v,
    tok_all,
    proj_send,
    proj_recv,
    gate_send,
    gate_recv,
    mixed_all,
    mixed_rows,
    att_all,
    res_rows,
    sq_send,
    sq_recv,
    up_send,
    up_recv,
    hid_all,
    hid_rows,
    down_send,
    down_recv,
    local_sem,
    tok_ssem,
    tok_rsem,
    proj_ssem,
    proj_rsem,
    gate_ssem,
    gate_rsem,
    mix_ssem,
    mix_rsem,
    att_ssem,
    att_rsem,
    sq_ssem,
    sq_rsem,
    up_ssem,
    up_rsem,
    hid_ssem,
    hid_rsem,
    down_ssem,
    down_rsem,
):
    kv, tp, D = cfg
    me, core = lax.axis_index("kv"), lax.axis_index("tp")
    S, H, HD, _ = state_mem.shape
    B = keys_blk.shape[2]
    width = H * HD
    rows, feats = tokens.shape
    total_rows = rows * tp
    chunks, _, _, chunk = up_send.shape

    loads = [
        pltpu.make_async_copy(a, b, local_sem.at[i])
        for i, (a, b) in enumerate(
            (
                (w_query, wq_v),
                (w_key, wk_v),
                (w_value, wv_v),
                (state_mem, state_v),
                (keys_blk, keys_v),
                (values_blk, values_v),
                (w_mixout, wo_v),
                (w_up, wu_v),
                (w_down, wd_v),
            )
        )
    ]
    for load in loads:
        load.start()

    barrier = pltpu.get_barrier_semaphore()

    def greet_kv(d, carry):
        pl.semaphore_signal(
            barrier, inc=1, device_id=(lax.rem(me + d, kv), core), device_id_type=MESH
        )
        return carry

    def greet_tp(d, carry):
        pl.semaphore_signal(
            barrier, inc=1, device_id=(me, lax.rem(core + d, tp)), device_id_type=MESH
        )
        return carry

    lax.fori_loop(1, tp, greet_tp, 0)
    lax.fori_loop(1, kv, greet_kv, 0)

    lane = lax.broadcasted_iota(jnp.int32, (H, 128), 1)
    sub = lax.broadcasted_iota(jnp.int32, (H, 128), 0)
    pick_i = (lane == sub).astype(F32).astype(BF16)
    pick_f = (lane == sub + H).astype(F32).astype(BF16)
    w_gates = (
        jnp.dot(w_igate[...], pick_i, preferred_element_type=F32)
        + jnp.dot(w_fgate[...], pick_f, preferred_element_type=F32)
    ).astype(BF16)

    row = lax.broadcasted_iota(jnp.int32, (S, 1), 0)
    length = jnp.zeros((S, 1), jnp.int32)
    for s in range(S):
        length = jnp.where(row == s, lengths[s], length)
    live = lax.broadcasted_iota(jnp.int32, (S, B), 1) < length
    later = (
        lax.broadcasted_iota(jnp.int32, (B, B), 0) > lax.broadcasted_iota(jnp.int32, (B, B), 1)
    ).astype(F32)
    base = []
    for h in range(H):
        forget = jnp.where(live, fgate_blk[:, h, :], 0.0)
        suffix = jnp.dot(
            forget, later, preferred_element_type=F32, precision=lax.Precision.HIGHEST
        )
        past = jnp.where(live, igate_blk[:, h, :] + suffix, -jnp.inf)
        carried = state_max[:, h : h + 1] + jnp.sum(forget, axis=1, keepdims=True)
        base.append((past, jnp.max(past, axis=1, keepdims=True), carried))
    pl.semaphore_wait(barrier, kv + tp - 2)

    def to_kv(d, src, dst, ssem, rsem):
        return pltpu.make_async_remote_copy(
            src_ref=src,
            dst_ref=dst,
            send_sem=ssem,
            recv_sem=rsem,
            device_id=(lax.rem(me + d, kv), core),
            device_id_type=MESH,
        )

    def to_tp(d, src, dst, ssem, rsem):
        return pltpu.make_async_remote_copy(
            src_ref=src,
            dst_ref=dst,
            send_sem=ssem,
            recv_sem=rsem,
            device_id=(me, lax.rem(core + d, tp)),
            device_id_type=MESH,
        )

    def each(n, make, act):
        def step(d, carry):
            act(make(d))
            return carry

        lax.fori_loop(1, n, step, 0)

    start = lambda copy: copy.start()
    wait_send = lambda copy: copy.wait_send()
    wait_recv = lambda copy: copy.wait_recv()


    inner = inner_size(kv)
    outer = kv // inner
    z, p = me // inner, lax.rem(me, inner)

    def at(dz, dp):
        return lax.rem(z + dz + outer, outer) * inner + lax.rem(p + dp + inner, inner)

    def remote(src, dst, ssem, rsem, target):
        return pltpu.make_async_remote_copy(
            src_ref=src,
            dst_ref=dst,
            send_sem=ssem,
            recv_sem=rsem,
            device_id=(target, core),
            device_id_type=MESH,
        )

    def rs_inner(send, recv, ssem, rsem, dz, dp):
        i = dz * inner + dp
        return remote(send(at(dz, dp)), recv(i), ssem(i), rsem(i), at(0, dp))

    def rs_outer(send, recv, ssem, rsem, dz):
        i = dz * inner
        return remote(send(at(dz, 0)), recv(i), ssem(i), rsem(i), at(dz, 0))

    def rs_start(refs):
        for dz in list(range(1, outer)) + [0]:
            each(inner, lambda dp, dz=dz: rs_inner(*refs, dz, dp), start)

    def rs_group(refs, dz):
        send, recv = refs[:2]

        def add(dp, total):
            rs_inner(*refs, dz, dp).wait_recv()
            return total + recv(dz * inner + dp)[...].astype(F32)

        return lax.fori_loop(1, inner, add, send(at(dz, 0))[...].astype(F32))

    def rs_middle(refs):
        send = refs[0]
        for dz in range(1, outer):
            send(at(dz, 0))[...] = rs_group(refs, dz).astype(BF16)
            rs_outer(*refs, dz).start()

    def rs_end(refs):
        recv = refs[1]

        def add(dz, total):
            rs_outer(*refs, dz).wait_recv()
            return total + recv(dz * inner)[...].astype(F32)

        return lax.fori_loop(1, outer, add, rs_group(refs, 0))

    def rs_close(refs):
        for dz in range(outer):
            each(inner, lambda dp, dz=dz: rs_inner(*refs, dz, dp), wait_send)
        each(outer, lambda dz: rs_outer(*refs, dz), wait_send)

    def ag_outer(block, ssem, rsem, dz, slot):
        i = dz * inner
        return remote(block(slot), block(slot), ssem(i), rsem(i), at(dz, 0))

    def ag_inner(block, ssem, rsem, dz, dp, slot):
        i = dz * inner + dp
        return remote(block(slot), block(slot), ssem(i), rsem(i), at(0, dp))

    def ag_start(refs):
        each(outer, lambda dz: ag_outer(*refs, dz, me), start)
        each(inner, lambda dp: ag_inner(*refs, 0, dp, me), start)

    def ag_relay(refs):
        for dz in range(1, outer):
            ag_outer(*refs, dz, at(-dz, 0)).wait_recv()
            each(inner, lambda dp, dz=dz: ag_inner(*refs, dz, dp, at(-dz, 0)), start)

    def ag_end(refs):
        for dz in range(outer):
            each(inner, lambda dp, dz=dz: ag_inner(*refs, dz, dp, at(-dz, -dp)), wait_recv)

    def ag_close(refs):
        each(outer, lambda dz: ag_outer(*refs, dz, me), wait_send)
        for dz in range(outer):
            each(inner, lambda dp, dz=dz: ag_inner(*refs, dz, dp, at(-dz, 0)), wait_send)

    def views(c, *refs):
        return tuple(lambda i, ref=ref: ref.at[c, i] for ref in refs)

    def tok_out(d):
        return to_tp(d, tokens, tok_all.at[core], tok_ssem.at[d], tok_rsem.at[d])

    def tok_in(d):
        slot = lax.rem(core - d + tp, tp)
        return to_tp(d, tokens, tok_all.at[slot], tok_ssem.at[d], tok_rsem.at[d])

    each(tp, tok_out, start)
    tok_all[core] = tokens[...]

    each(tp, tok_in, wait_recv)
    widened = tok_all[...].astype(F32).reshape(total_rows, feats)
    square_in = jnp.sum(widened * widened, axis=1, keepdims=True)
    scaled_in = (widened * gain_mix[...]).astype(BF16)

    gates = jnp.dot(scaled_in, w_gates, preferred_element_type=F32)
    lane_r = lax.broadcasted_iota(jnp.int32, gates.shape, 1)
    gates = jnp.where(lane_r == 2 * H, square_in, gates)
    for j in range(kv):
        gate_send[j] = gates[j * S : (j + 1) * S]

    def gate_out(d):
        return to_kv(
            d, gate_send.at[lax.rem(me + d, kv)], gate_recv.at[d], gate_ssem.at[d], gate_rsem.at[d]
        )

    each(kv, gate_out, start)

    proj_refs = [views(i, proj_send, proj_recv, proj_ssem, proj_rsem) for i in range(1)]
    for i, w in enumerate((wq_v, wk_v, wv_v)):
        loads[i].wait()
        part = jnp.dot(scaled_in, w[...], preferred_element_type=F32)
        for j in range(kv):
            proj_send[0, j, :, i * width : (i + 1) * width] = part[j * S : (j + 1) * S].astype(BF16)
    rs_start(proj_refs[0])

    for refs in proj_refs:
        rs_middle(refs)
    loads[3].wait()

    def split(i, carry):
        s, h = i // H, lax.rem(i, H)
        full = state_v[s, h]
        hi = full.astype(BF16)
        state_hi[s, h] = hi
        state_lo[s, h] = (full - hi.astype(F32)).astype(BF16)
        return carry

    lax.fori_loop(0, S * H, split, 0)
    loads[4].wait()
    loads[5].wait()

    def gate_add(d, total):
        gate_out(d).wait_recv()
        return total + gate_recv[d]

    gate_sum = lax.fori_loop(1, kv, gate_add, gate_send[me])
    factor_in = lax.rsqrt(gate_sum[:, 2 * H : 2 * H + 1] / D + EPS)
    gate_sum = gate_sum * factor_in

    projected = (rs_end(proj_refs[0]) * factor_in).astype(BF16)
    query, key_new, value_new = (projected[:, i * width : (i + 1) * width] for i in range(3))

    scale = HD ** (-0.5)
    contract = (((1,), (1,)), ((), ()))
    mixed = []
    for h in range(H):
        cols = slice(h * HD, (h + 1) * HD)
        q, k, v = query[:, cols], key_new[:, cols], value_new[:, cols]
        past, past_top, carried = base[h]
        ig = gate_sum[:, h : h + 1] + bias_igate[h]
        raw = gate_sum[:, H + h : H + h + 1] + bias_fgate[h]
        fg = jnp.minimum(raw, 0.0) - jnp.log1p(jnp.exp(-jnp.abs(raw)))
        carried = carried + fg
        top = jnp.maximum(jnp.maximum(carried, ig), past_top + fg)
        decay = jnp.exp(past + (fg - top))
        scores = jnp.zeros((S, B), F32)
        state_term = jnp.zeros((S, HD), F32)
        for s in range(S):
            mine = row == s
            got = lax.dot_general(q, keys_v[s, h], contract, preferred_element_type=F32)
            scores = jnp.where(mine, got, scores)
            mem = lax.dot_general(
                q, state_hi[s, h], contract, preferred_element_type=F32
            ) + lax.dot_general(q, state_lo[s, h], contract, preferred_element_type=F32)
            state_term = jnp.where(mine, mem, state_term)
        weights = (decay * (scores * scale)).astype(BF16)
        block_term = jnp.zeros((S, HD), F32)
        for s in range(S):
            got = jnp.dot(weights, values_v[s, h], preferred_element_type=F32)
            block_term = jnp.where(row == s, got, block_term)
        own = jnp.sum(q.astype(F32) * k.astype(F32), axis=1, keepdims=True) * scale
        numerator = (
            state_term * jnp.exp(carried - top)
            + block_term
            + (jnp.exp(ig - top) * own) * v.astype(F32)
        )
        spread = jnp.mean(numerator * numerator, axis=1, keepdims=True)
        mixed_all[me, :, cols] = (numerator * lax.rsqrt(spread + EPS) * gain_head[...]).astype(BF16)

    def mix_out(d):
        return to_kv(d, mixed_all.at[me], mixed_all.at[me], mix_ssem.at[d], mix_rsem.at[d])

    def mix_in(d):
        slot = lax.rem(me - d + kv, kv)
        return to_kv(d, mixed_all.at[me], mixed_all.at[slot], mix_ssem.at[d], mix_rsem.at[d])

    each(kv, mix_out, start)
    for i in (6, 7, 8):
        loads[i].wait()
    each(kv, mix_in, wait_recv)
    for j in range(kv):
        mixed_rows[j * S : (j + 1) * S] = mixed_all[j].astype(F32)
    att_all[core] = jnp.dot(
        mixed_rows[...].astype(BF16), wo_v[...], preferred_element_type=F32
    ).astype(BF16)

    def att_out(d):
        return to_tp(d, att_all.at[core], att_all.at[core], att_ssem.at[d], att_rsem.at[d])

    def att_in(d):
        slot = lax.rem(core - d + tp, tp)
        return to_tp(d, att_all.at[core], att_all.at[slot], att_ssem.at[d], att_rsem.at[d])

    each(tp, att_out, start)
    each(tp, att_in, wait_recv)
    attended = att_all[0].astype(F32)
    for t in range(1, tp):
        attended = attended + att_all[t].astype(F32)
    restored = (widened + attended).astype(BF16).astype(F32)
    res_rows[...] = restored.reshape(tp, rows, feats)
    square_mid = jnp.sum(restored * restored, axis=1, keepdims=True)
    square_wide = jnp.broadcast_to(square_mid, (total_rows, 128))
    for j in range(kv):
        sq_send[j] = square_wide[j * S : (j + 1) * S]

    def sq_out(d):
        return to_kv(
            d, sq_send.at[lax.rem(me + d, kv)], sq_recv.at[d], sq_ssem.at[d], sq_rsem.at[d]
        )

    each(kv, sq_out, start)
    scaled_mid = (restored * gain_mlp[...]).astype(BF16)

    up_refs = [views(c, up_send, up_recv, up_ssem, up_rsem) for c in range(chunks)]
    hid_refs = [views(c, hid_all, hid_ssem, hid_rsem) for c in range(chunks)]

    for c in range(chunks):
        part = jnp.dot(
            scaled_mid, wu_v[:, c * chunk : (c + 1) * chunk], preferred_element_type=F32
        )
        for j in range(kv):
            up_send[c, j] = part[j * S : (j + 1) * S].astype(BF16)
        rs_start(up_refs[c])

    def sq_add(d, total):
        sq_out(d).wait_recv()
        return total + sq_recv[d]

    square_sum = lax.fori_loop(1, kv, sq_add, sq_send[me])
    factor_mid = lax.rsqrt(square_sum[:, 0:1] / D + EPS)

    for refs in up_refs:
        rs_middle(refs)
    for c in range(chunks):
        active = jnp.maximum(rs_end(up_refs[c]) * factor_mid, 0.0)
        hid_all[c, me] = (active * active).astype(BF16)
        ag_start(hid_refs[c])
        if c > 0:
            ag_relay(hid_refs[c - 1])
    ag_relay(hid_refs[-1])

    down = jnp.zeros((total_rows, feats), F32)
    for c in range(chunks):
        ag_end(hid_refs[c])
        for j in range(kv):
            hid_rows[j * S : (j + 1) * S] = hid_all[c, j].astype(F32)
        down = down + jnp.dot(
            hid_rows[...].astype(BF16),
            wd_v[c * chunk : (c + 1) * chunk],
            preferred_element_type=F32,
        )
    down_send[...] = down.astype(BF16).reshape(tp, rows, feats)

    def down_out(d):
        return to_tp(
            d, down_send.at[lax.rem(core + d, tp)], down_recv.at[d], down_ssem.at[d], down_rsem.at[d]
        )

    each(tp, down_out, start)

    each(tp, tok_out, wait_send)
    each(kv, gate_out, wait_send)
    for refs in proj_refs + up_refs:
        rs_close(refs)
    for refs in hid_refs:
        ag_close(refs)
    each(kv, mix_out, wait_send)
    each(tp, att_out, wait_send)
    each(kv, sq_out, wait_send)

    def down_add(d, total):
        down_out(d).wait_recv()
        return total + down_recv[d].astype(F32)

    total = lax.fori_loop(1, tp, down_add, down_send[core].astype(F32))
    out[...] = (res_rows[core] + total).astype(out.dtype)
    each(tp, down_out, wait_send)


def body(kv, tp, *args):
    (
        tokens,
        gain_mix,
        w_query,
        w_key,
        w_value,
        w_igate,
        w_fgate,
        bias_igate,
        bias_fgate,
        state_mem,
        state_max,
        keys_blk,
        values_blk,
        igate_blk,
        fgate_blk,
        lengths,
        gain_head,
        w_mixout,
        gain_mlp,
        w_up,
        w_down,
    ) = args
    rows, feats = tokens.shape
    S, H, HD, _ = state_mem.shape
    width = H * HD
    hidden = w_up.shape[1]
    chunks = ceil_chunks(hidden)
    chunk = hidden // chunks
    vm = pl.BlockSpec(memory_space=pltpu.VMEM)
    sm = pl.BlockSpec(memory_space=pltpu.SMEM)
    hbm = pl.BlockSpec(memory_space=pl.ANY)
    in_specs = [
        vm,
        vm,
        hbm,
        hbm,
        hbm,
        vm,
        vm,
        sm,
        sm,
        hbm,
        vm,
        hbm,
        hbm,
        vm,
        vm,
        sm,
        vm,
        hbm,
        vm,
        hbm,
        hbm,
    ]
    V = pltpu.VMEM
    dma = pltpu.SemaphoreType.DMA
    scratch = [
        V(w_query.shape, BF16),
        V(w_key.shape, BF16),
        V(w_value.shape, BF16),
        V(state_mem.shape, F32),
        V(state_mem.shape, BF16),
        V(state_mem.shape, BF16),
        V(keys_blk.shape, BF16),
        V(values_blk.shape, BF16),
        V(w_mixout.shape, BF16),
        V(w_up.shape, BF16),
        V(w_down.shape, BF16),
        V((tp, rows, feats), BF16),
        V((1, kv, S, 3 * width), BF16),
        V((1, kv, S, 3 * width), BF16),
        V((kv, S, 128), F32),
        V((kv, S, 128), F32),
        V((kv, S, width), BF16),
        V((kv * S, width), F32),
        V((tp, kv * S, feats), BF16),
        V((tp, rows, feats), F32),
        V((kv, S, 128), F32),
        V((kv, S, 128), F32),
        V((chunks, kv, S, chunk), BF16),
        V((chunks, kv, S, chunk), BF16),
        V((chunks, kv, S, chunk), BF16),
        V((kv * S, chunk), F32),
        V((tp, rows, feats), BF16),
        V((tp, rows, feats), BF16),
        dma((9,)),
        dma((tp,)),
        dma((tp,)),
        dma((1, kv)),
        dma((1, kv)),
        dma((kv,)),
        dma((kv,)),
        dma((kv,)),
        dma((kv,)),
        dma((tp,)),
        dma((tp,)),
        dma((kv,)),
        dma((kv,)),
        dma((chunks, kv)),
        dma((chunks, kv)),
        dma((chunks, kv)),
        dma((chunks, kv)),
        dma((tp,)),
        dma((tp,)),
    ]
    return pl.pallas_call(
        functools.partial(kernel, (kv, tp, kv * feats)),
        out_shape=jax.ShapeDtypeStruct((rows, feats), BF16),
        in_specs=in_specs,
        out_specs=vm,
        scratch_shapes=scratch,
        compiler_params=pltpu.CompilerParams(
            collective_id=0, has_side_effects=True, vmem_limit_bytes=56 * 1024 * 1024
        ),
    )(
        tokens,
        gain_mix.reshape(1, -1),
        w_query,
        w_key,
        w_value,
        w_igate,
        w_fgate,
        bias_igate,
        bias_fgate,
        state_mem,
        state_max,
        keys_blk,
        values_blk,
        igate_blk,
        fgate_blk,
        lengths,
        gain_head.reshape(1, -1),
        w_mixout,
        gain_mlp.reshape(1, -1),
        w_up,
        w_down,
    )


def solution(mesh):
    in_specs = (
        P("tp", "kv"),
        P("kv"),
        P("kv", "tp"),
        P("kv", "tp"),
        P("kv", "tp"),
        P("kv", "tp"),
        P("kv", "tp"),
        P("tp"),
        P("tp"),
        P("kv", "tp", None, None),
        P("kv", "tp"),
        P("kv", "tp", None, None),
        P("kv", "tp", None, None),
        P("kv", "tp", None),
        P("kv", "tp", None),
        P("kv"),
        P(),
        P("tp", "kv"),
        P("kv"),
        P("kv", "tp"),
        P("tp", "kv"),
    )
    out_specs = P("tp", "kv")
    run = functools.partial(body, mesh.shape["kv"], mesh.shape["tp"])
    return jax.shard_map(run, mesh=mesh, in_specs=in_specs, out_specs=out_specs, check_vma=False)
```

profile of v0, /device:TPU:0, one launch (start us, length us, event | category | flops | bytes accessed | tf_op | source)
XLA Modules:
  0.0 53.0 jit_solution(6419289001698820024)
XLA Ops:
  0.0 1.4 %copy.22.w_igate = bf16[128,4]{1,0:T(8,128)(2,1)} copy(bf16[128,4]{0,1:T(4,128)(2,1)} %param.26) | data formatting | bytes 2048 | tf_op args[5]
  1.4 1.4 %copy.23.w_fgate = bf16[128,4]{1,0:T(8,128)(2,1)} copy(bf16[128,4]{0,1:T(4,128)(2,1)} %param.27) | data formatting | bytes 2048 | tf_op args[6]
  2.8 48.9 %shard_map.199 = bf16[32,128]{1,0:T(8,128)(2,1)} custom-call(bf16[32,128]{1,0:T(8,128)(2,1)} %tokens.1, f32[1,128]{1,0:T(1,128)} %bitcast.4, bf16[128,1024]{1,0:T(8,128)(2,1)} %w_query.1, bf16[128,1024]{1,0:T(8,128)(2,1)} %w_key.1, bf16[128,1024]{1,0:T(8,128)(2,1)} %w_value.1, bf16[128,4]{1,0:T(8,128)(2,1)} %copy.22.w_igate, bf16[128,4]{1,0:T(8,128)(2,1)} %copy.23.w_fgate, ...), custom_call_target="tpu_custom_call" | custom-call | tf_op jit(solution)/shard_map/pallas_call | solution.py:604
  51.7 1.3 %copy.25 = bf16[32,128]{1,0:T(8,128)(2,1)} copy(bf16[32,128]{1,0:T(8,128)(2,1)} %shard_map.199) | data formatting | bytes 16384
where the time goes:
time: 53.3 us; the launch traced here: 53 us
  Pallas kernels  48.9 us (92%)
  local copies, waits for them, and re-layouts  4.08 us (8%)
    pallas_call x1, Pallas kernels, body(): pl.pallas_call(functools.partial(kernel, (kv, tp, kv * feats)), out_shape...  48.9 us
    unnamed x3, local copies, waits for them, and re-layouts  4.08 us

commit v1 on v0

--- a/solution.py
+++ b/solution.py
@@ -1,4 +1,6 @@
 import functools
+from types import SimpleNamespace
+
 import jax
 import jax.numpy as jnp
 from jax import lax
@@ -20,7 +22,7 @@
     return max(d for d in range(1, count + 1) if count % d == 0 and d * d <= count)
 
 
-def kernel(
+def any_kernel(
     cfg,
     tokens,
     gain_mix,
@@ -494,7 +496,7 @@
     each(tp, down_out, wait_send)
 
 
-def body(kv, tp, *args):
+def any_body(kv, tp, *args):
     (
         tokens,
         gain_mix,
@@ -602,7 +604,7 @@
         dma((tp,)),
     ]
     return pl.pallas_call(
-        functools.partial(kernel, (kv, tp, kv * feats)),
+        functools.partial(any_kernel, (kv, tp, kv * feats)),
         out_shape=jax.ShapeDtypeStruct((rows, feats), BF16),
         in_specs=in_specs,
         out_specs=vm,
@@ -635,6 +637,697 @@
     )
 
 
+def flip(index, mask):
+    bit = 1
+    while bit <= mask:
+        if mask & bit:
+            index = index + bit * (1 - 2 * lax.rem(lax.div(index, bit), 2))
+        bit *= 2
+    return index
+
+
+def stages(kv):
+    inner = inner_size(kv)
+    outer = kv // inner
+    if (inner, outer) != (4, 4):
+        return (([m for m in range(inner)], [m * inner for m in range(outer)]),)
+    ways = (((1, 2), (4, 8)), ((1, 4), (2, 8)), ((2, 4), (1, 8)))
+    return tuple(tuple([0, a, b, a + b] for a, b in way) for way in ways)
+
+
+def kernel(cfg, names, *refs):
+    kv, tp, D = cfg
+    r = SimpleNamespace(**dict(zip(names, refs, strict=True)))
+    me, core = lax.axis_index("kv"), lax.axis_index("tp")
+    inner = inner_size(kv)
+    outer = kv // inner
+    other = 1 - core
+    ways = stages(kv)
+
+    def split(way):
+        def place(masks):
+            total, step = 0, 1
+            while step < len(masks):
+                total = total + step * lax.rem(lax.div(me, masks[step]), 2)
+                step *= 2
+            return total
+
+        return place(way[1]), place(way[0])
+    S, H, HD, _ = r.state_mem.shape
+    B = r.fgate_blk.shape[2]
+    width = H * HD
+    R, F = r.tokens.shape
+    per = kv // tp
+    half = lax.div(me, per)
+    jj_me = lax.rem(me, per)
+    chunks, _, _, CW = r.up_send.shape
+    proj_way = [ways[a % len(ways)] for a in range(3)]
+    up_way = [ways[c % len(ways)] for c in range(chunks)]
+
+    barrier = pltpu.get_barrier_semaphore()
+
+    def greet(target, c):
+        pl.semaphore_signal(barrier, inc=1, device_id=(target, c), device_id_type=MESH)
+
+    for m in reversed(range(1, kv)):
+        target = flip(me, m)
+        greet(target, core)
+        greet(target, other)
+    greet(me, other)
+
+    taken = iter(range(r.local_sem.shape[0]))
+
+    def load(whole, *pieces):
+        sem = r.local_sem.at[next(taken)]
+        for i, piece in enumerate(pieces):
+            dst = whole if len(pieces) == 1 else whole.at[i]
+            pltpu.make_async_copy(piece, dst, sem).start()
+        return pltpu.make_async_copy(whole, whole, sem)
+
+    got_tokens = load(r.v_tokens, r.tokens)
+    got_gain_mix = load(r.v_gain_mix, r.gain_mix)
+    got_w_gate = load(r.v_w_gate, r.w_igate, r.w_fgate)
+    got_w_qkv = load(r.v_w_qkv, r.w_query, r.w_key, r.w_value)
+    got_blk = [
+        load(r.v_gate_blk, r.fgate_blk, r.igate_blk),
+        load(r.v_lengths, r.lengths),
+        load(r.v_state_max, r.state_max),
+        load(r.v_bias, r.bias_igate, r.bias_fgate),
+    ]
+    got_memory = [
+        load(r.v_state_mem, r.state_mem),
+        load(r.v_kv_blk, r.keys_blk, r.values_blk),
+        load(r.v_gain_head, r.gain_head),
+    ]
+    got_gain_mlp = load(r.v_gain_mlp, r.gain_mlp)
+    got_w_mixout = load(r.v_w_mixout.at[0], r.w_mixout)
+    got_w_up = load(r.v_w_up.at[0], r.w_up)
+    got_w_down = load(r.v_w_down.at[0], r.w_down)
+
+    def loaded(copies):
+        for copy in copies:
+            copy.wait()
+
+    def remote(src, dst, ssem, rsem, target, c):
+        return pltpu.make_async_remote_copy(
+            src_ref=src,
+            dst_ref=dst,
+            send_sem=ssem,
+            recv_sem=rsem,
+            device_id=(target, c),
+            device_id_type=MESH,
+        )
+
+    def drain(ref, sem):
+        remote(ref, ref, sem, sem, me, other).wait_send()
+
+    loaded([got_tokens, got_gain_mix, got_w_gate])
+    lane = lax.broadcasted_iota(jnp.int32, (H, 128), 1)
+    sub = lax.broadcasted_iota(jnp.int32, (H, 128), 0)
+    pick_i = (lane == sub).astype(F32).astype(BF16)
+    pick_f = (lane == sub + H).astype(F32).astype(BF16)
+    first = (((0,), (0,)), ((), ()))
+    w_gates = (
+        lax.dot_general(r.v_w_gate[0], pick_i, first, preferred_element_type=F32)
+        + lax.dot_general(r.v_w_gate[1], pick_f, first, preferred_element_type=F32)
+    ).astype(BF16)
+    lane_r = lax.broadcasted_iota(jnp.int32, (R, 128), 1)
+    gain_mix = r.v_gain_mix[...]
+    gate_send = r.gate_send
+    proj_send, proj_recv, proj_mid, proj_last = r.proj_send, r.proj_recv, r.proj_mid, r.proj_last
+
+    def project(rows, group):
+        scaled = (rows * gain_mix).astype(BF16)
+        square = jnp.sum(rows * rows, axis=1, keepdims=True)
+        gates = jnp.dot(scaled, w_gates, preferred_element_type=F32)
+        gates = jnp.where(lane_r == 2 * H, square, gates)
+        for jj in range(per):
+            gate_send[group * per + jj] = gates[jj * S : (jj + 1) * S]
+        for i in range(3):
+            part = jnp.dot(scaled, r.v_w_qkv[i], preferred_element_type=F32)
+            for jj in range(per):
+                proj_send[i, group * per + jj] = part[jj * S : (jj + 1) * S].astype(BF16)
+
+    own_rows = r.v_tokens[...].astype(F32)
+    got_w_qkv.wait()
+    project(own_rows, core)
+
+    loaded(got_blk)
+    row = lax.broadcasted_iota(jnp.int32, (S, 1), 0)
+    eye_s = lax.broadcasted_iota(jnp.int32, (S, S), 0) == lax.broadcasted_iota(jnp.int32, (S, S), 1)
+    length = jnp.sum(
+        jnp.where(eye_s, r.v_lengths[...].astype(F32), 0.0), axis=1, keepdims=True
+    )
+    live = lax.broadcasted_iota(jnp.int32, (S, B), 1).astype(F32) < length
+    later = (
+        lax.broadcasted_iota(jnp.int32, (B, B), 0) > lax.broadcasted_iota(jnp.int32, (B, B), 1)
+    ).astype(F32)
+    base = []
+    for h in range(H):
+        forget = jnp.where(live, r.v_gate_blk[0, :, h, :], 0.0)
+        suffix = jnp.dot(
+            forget, later, preferred_element_type=F32, precision=lax.Precision.HIGHEST
+        )
+        past = jnp.where(live, r.v_gate_blk[1, :, h, :] + suffix, -jnp.inf)
+        carried = r.v_state_max[:, h : h + 1] + jnp.sum(forget, axis=1, keepdims=True)
+        base.append((past, jnp.max(past, axis=1, keepdims=True), carried))
+    pl.semaphore_wait(barrier, kv * tp - 1)
+
+    tok_copy = remote(
+        r.v_tokens, r.tok_peer, r.pair_ssem.at[0], r.pair_rsem.at[0], me, other
+    )
+    tok_copy.start()
+
+    def pair(i, ref):
+        return remote(ref.at[0], ref.at[1], r.pair_ssem.at[i], r.pair_rsem.at[i], me, other)
+
+    pairs = [pair(1, r.v_w_mixout), pair(2, r.v_w_up), pair(3, r.v_w_down)]
+
+    def proj_one(a, mz, mp):
+        first, second = proj_way[a]
+        return remote(
+            proj_send.at[a, flip(me, first[mp] + second[mz])],
+            proj_recv.at[a, mz, mp],
+            r.proj_ssem,
+            r.proj_rsem.at[a, mz // (outer // 2)],
+            flip(me, first[mp]),
+            other,
+        )
+
+    def proj_two(a, mz):
+        return remote(
+            proj_mid.at[a, mz],
+            proj_last.at[a, mz],
+            r.mid_ssem.at[0],
+            r.mid_rsem.at[a],
+            flip(me, proj_way[a][1][mz]),
+            other,
+        )
+
+    far = [mz for mz in reversed(range(outer)) if mz >= outer // 2]
+    near = [mz for mz in reversed(range(outer)) if mz < outer // 2]
+    peers = list(reversed(range(inner)))
+
+    def send_groups(a, groups):
+        for mz in groups:
+            for mp in peers:
+                proj_one(a, mz, mp).start()
+
+    def gate_copy(m):
+        return remote(
+            gate_send.at[flip(me, m)],
+            r.gate_recv.at[m],
+            r.gate_ssem,
+            r.gate_rsem,
+            flip(me, m),
+            core,
+        )
+
+    far_m = [m for m in reversed(range(1, kv)) if m >= per]
+    near_m = [m for m in reversed(range(1, kv)) if m < per]
+
+    @pl.when(core != half)
+    def _():
+        for m in far_m:
+            gate_copy(m).start()
+        for a in range(3):
+            send_groups(a, far)
+
+    tok_copy.wait_recv()
+    peer_rows = r.tok_peer[...].astype(F32)
+    project(peer_rows, other)
+
+    @pl.when(core == half)
+    def _():
+        for m in far_m:
+            gate_copy(m).start()
+        send_groups(0, far)
+
+    for m in near_m:
+        gate_copy(m).start()
+    send_groups(0, near)
+
+    @pl.when(core == half)
+    def _():
+        for a in (1, 2):
+            send_groups(a, far)
+
+    for a in (1, 2):
+        send_groups(a, near)
+
+    got_w_mixout.wait()
+    pairs[0].start()
+
+    loaded(got_memory)
+
+    def narrow(i, carry):
+        s, h = lax.div(i, H), lax.rem(i, H)
+        r.state_t[s, h] = r.v_state_mem[s, h].T.astype(BF16)
+        r.keys_t[s, h] = r.v_kv_blk[0, s, h].T
+        return carry
+
+    lax.fori_loop(0, S * H, narrow, 0)
+
+    def summed(ref):
+        total = ref[0].astype(F32)
+        for i in range(1, ref.shape[0]):
+            total = total + ref[i].astype(F32)
+        return total
+
+    def proj_middle(a):
+        for side, groups in ((1, far), (0, near)):
+            drain(
+                proj_recv.at[a, pl.ds(side * (outer // 2), outer // 2)], r.proj_rsem.at[a, side]
+            )
+            for mz in groups:
+                proj_mid[a, mz] = summed(proj_recv.at[a, mz]).astype(BF16)
+                proj_two(a, mz).start()
+
+    def proj_end(a):
+        drain(proj_last.at[a], r.mid_rsem.at[a])
+        return (summed(proj_last.at[a]) * factor_in).astype(BF16)
+
+    proj_middle(0)
+    proj_middle(1)
+    proj_middle(2)
+    got_w_up.wait()
+    pairs[1].start()
+    drain(r.gate_recv.at[pl.ds(1, kv - 1)], r.gate_rsem)
+    gate_sum = gate_send[me]
+    for m in range(1, kv):
+        gate_sum = gate_sum + r.gate_recv[m]
+    factor_in = lax.rsqrt(gate_sum[:, 2 * H : 2 * H + 1] / D + EPS)
+    gate_sum = gate_sum * factor_in
+    query = proj_end(0)
+
+    scale = HD ** (-0.5)
+    cells = []
+    for h in range(H):
+        q = query[:, h * HD : (h + 1) * HD]
+        past, past_top, carried = base[h]
+        ig = gate_sum[:, h : h + 1] + r.v_bias[0, :, h : h + 1]
+        raw = gate_sum[:, H + h : H + h + 1] + r.v_bias[1, :, h : h + 1]
+        fg = jnp.minimum(raw, 0.0) - jnp.log1p(jnp.exp(-jnp.abs(raw)))
+        carried = carried + fg
+        top = jnp.maximum(jnp.maximum(carried, ig), past_top + fg)
+        decay = jnp.exp(past + (fg - top))
+        scores = jnp.zeros((S, B), F32)
+        state_term = jnp.zeros((S, HD), F32)
+        for s in range(S):
+            mine = row == s
+            got = jnp.dot(q, r.keys_t[s, h], preferred_element_type=F32)
+            scores = jnp.where(mine, got, scores)
+            mem = jnp.dot(q, r.state_t[s, h], preferred_element_type=F32)
+            state_term = jnp.where(mine, mem, state_term)
+        weights = (decay * (scores * scale)).astype(BF16)
+        block_term = jnp.zeros((S, HD), F32)
+        for s in range(S):
+            got = jnp.dot(weights, r.v_kv_blk[1, s, h], preferred_element_type=F32)
+            block_term = jnp.where(row == s, got, block_term)
+        cells.append((state_term * jnp.exp(carried - top) + block_term, jnp.exp(ig - top)))
+
+    key_new = proj_end(1)
+    value_new = proj_end(2)
+    for h in range(H):
+        cols = slice(h * HD, (h + 1) * HD)
+        q, k, v = query[:, cols], key_new[:, cols], value_new[:, cols]
+        older, entering = cells[h]
+        own = jnp.sum(q.astype(F32) * k.astype(F32), axis=1, keepdims=True) * scale
+        numerator = older + (entering * own) * v.astype(F32)
+        spread = jnp.mean(numerator * numerator, axis=1, keepdims=True)
+        r.mixed_own[:, cols] = (
+            numerator * lax.rsqrt(spread + EPS) * r.v_gain_head[...]
+        ).astype(BF16)
+
+    mixed_all = r.mixed_all
+    slot = lax.rem(half + core, 2)
+    mine_at = slot * per + jj_me
+
+    def mix_copy(m):
+        return remote(
+            r.mixed_own,
+            mixed_all.at[mine_at],
+            r.mix_ssem,
+            r.mix_rsem,
+            flip(me, m),
+            half,
+        )
+
+    for m in reversed(range(1, kv)):
+        mix_copy(m).start()
+
+    @pl.when(slot == 1)
+    def _():
+        mix_copy(0).start()
+
+    @pl.when(slot == 0)
+    def _():
+        mixed_all[mine_at] = r.mixed_own[...]
+
+    loaded([got_w_down, got_gain_mlp])
+    pairs[0].wait()
+
+    @pl.when(half == core)
+    def _():
+        drain(mixed_all.at[pl.ds(0, kv - 1)], r.mix_rsem)
+
+    @pl.when(half != core)
+    def _():
+        drain(mixed_all, r.mix_rsem)
+
+    mixed_rows = r.mixed_rows
+    attended = jnp.zeros((R, F), F32)
+    for c in range(tp):
+        for jj in range(per):
+            mixed_rows[jj * S : (jj + 1) * S, c * width : (c + 1) * width] = mixed_all[
+                c * per + jj
+            ].astype(F32)
+        attended = attended + jnp.dot(
+            mixed_rows[:, c * width : (c + 1) * width].astype(BF16),
+            r.v_w_mixout[c],
+            preferred_element_type=F32,
+        ).astype(BF16).astype(F32)
+
+    restored = (own_rows + attended).astype(BF16).astype(F32)
+    r.res_rows[...] = restored
+    scaled_mid = (restored * r.v_gain_mlp[...]).astype(BF16)
+
+    up_send, up_recv, up_mid, up_last = r.up_send, r.up_recv, r.up_mid, r.up_last
+
+    def up_one(c, mz, mp):
+        place = split(up_way[c])
+        return remote(
+            up_send.at[c, flip(place[0], mz) * inner + flip(place[1], mp)],
+            up_recv.at[c, mz, mp],
+            r.up_ssem,
+            r.up_rsem.at[c, mz // (outer // 2)],
+            flip(me, up_way[c][0][mp]),
+            other,
+        )
+
+    def up_two(c, mz):
+        return remote(
+            up_mid.at[c, mz],
+            up_last.at[c, mz],
+            r.mid_ssem.at[1],
+            r.up_lsem.at[c],
+            flip(me, up_way[c][1][mz]),
+            other,
+        )
+
+    parts = chunks // tp
+    span = kv * CW
+
+    def up_start(c, groups):
+        for mz in groups:
+            for mp in peers:
+                up_one(c, mz, mp).start()
+
+    def up_compute(c):
+        if c == parts:
+            pairs[1].wait()
+        begin = (c % parts) * span
+        part = jnp.dot(
+            scaled_mid,
+            r.v_w_up[c // parts, :, begin : begin + span],
+            preferred_element_type=F32,
+        ).astype(BF16)
+        for j in range(kv):
+            up_send[c, j] = part[:, j * CW : (j + 1) * CW]
+
+    plan = [(c, side) for c in range(chunks) for side in (1, 0)]
+    for i, (c, side) in enumerate(plan):
+        if c not in [x for x, _ in plan[:i]]:
+            up_compute(c)
+        up_start(c, far if side else near)
+    pairs[2].start()
+
+    square_mid = jnp.sum(restored * restored, axis=1, keepdims=True)
+    eye_r = lax.broadcasted_iota(jnp.int32, (R, 128), 0) == lane_r
+    r.sq_all[0] = jnp.sum(jnp.where(eye_r, square_mid, 0.0), axis=0, keepdims=True)
+
+    def sq_copy(m):
+        return remote(
+            r.sq_all.at[0],
+            r.sq_all.at[m],
+            r.sq_ssem,
+            r.sq_rsem,
+            flip(me, m),
+            core,
+        )
+
+    for m in reversed(range(1, kv)):
+        sq_copy(m).start()
+
+    def up_middle(c, side):
+        drain(up_recv.at[c, pl.ds(side * (outer // 2), outer // 2)], r.up_rsem.at[c, side])
+        for mz in far if side else near:
+            up_mid[c, mz] = summed(up_recv.at[c, mz]).astype(BF16)
+            up_two(c, mz).start()
+
+    hid_mid, hid_all = r.hid_mid, r.hid_all
+
+    def hid_near(c, mp):
+        mine = hid_all.at[c, 0, split(up_way[c])[1]]
+        return remote(
+            mine,
+            mine,
+            r.hid_ssem.at[2],
+            r.hid_rsem.at[c],
+            flip(me, up_way[c][0][mp]),
+            core,
+        )
+
+    def hid_one(c, mz):
+        return remote(
+            hid_all.at[c, 0, split(up_way[c])[1]],
+            hid_mid.at[c, mz],
+            r.hid_ssem.at[0],
+            r.hid_msem.at[c, mz - 1],
+            flip(me, up_way[c][1][mz]),
+            other,
+        )
+
+    def hid_two(c, mz, mp):
+        return remote(
+            hid_mid.at[c, mz],
+            hid_all.at[c, mz, split(up_way[c])[1]],
+            r.hid_ssem.at[1],
+            r.hid_rsem.at[c],
+            flip(me, up_way[c][0][mp]),
+            other,
+        )
+
+    def hid_start(c):
+        drain(up_last.at[c], r.up_lsem.at[c])
+        active = jnp.maximum(summed(up_last.at[c]), 0.0)
+        hid_all[c, 0, split(up_way[c])[1]] = (active * active).astype(BF16)
+        for mz in reversed(range(1, outer)):
+            hid_one(c, mz).start()
+        for mp in peers[:-1]:
+            hid_near(c, mp).start()
+
+    def hid_relay(c, mz):
+        drain(hid_mid.at[c, mz], r.hid_msem.at[c, mz - 1])
+        for mp in peers:
+            hid_two(c, mz, mp).start()
+
+    def hops(mz):
+        return 1.8 + 0.7 * ((mz & 1) + 2 * (mz >> 1)) if mz else 0.9
+
+    steps, ready = [], [0.0] * chunks
+    for i, (c, side) in enumerate(plan):
+        due = 3.2 * (i + 1) / len(plan) + 2.8
+        steps.append((due, up_middle, c, side))
+        ready[c] = max([ready[c], *(due + hops(mz) for mz in (far if side else near))])
+    for c in range(chunks):
+        steps.append((ready[c] + 0.2, hid_start, c))
+        for mz in range(1, outer):
+            steps.append((ready[c] + 0.4 + hops(mz), hid_relay, c, mz))
+    order = [step[1:] for step in sorted(steps, key=lambda step: step[0])]
+    for step, *which in order:
+        step(*which)
+
+    tok_copy.wait_send()
+    drain(r.gate_recv.at[pl.ds(1, kv - 1)], r.gate_ssem)
+    drain(proj_recv, r.proj_ssem)
+    drain(proj_last, r.mid_ssem.at[0])
+
+    @pl.when(slot == 0)
+    def _():
+        drain(mixed_all.at[pl.ds(0, kv - 1)], r.mix_ssem)
+
+    @pl.when(slot == 1)
+    def _():
+        drain(mixed_all, r.mix_ssem)
+
+    drain(r.sq_all.at[pl.ds(1, kv - 1)], r.sq_ssem)
+    drain(up_recv, r.up_ssem)
+    drain(up_last, r.mid_ssem.at[1])
+    pairs[2].wait()
+    drain(r.sq_all.at[pl.ds(1, kv - 1)], r.sq_rsem)
+    squares = r.sq_all[0]
+    for m in range(1, kv):
+        squares = squares + r.sq_all[m]
+    square_sum = jnp.sum(jnp.where(eye_r, squares, 0.0), axis=1, keepdims=True)
+    factor_mid = lax.rsqrt(square_sum / D + EPS)
+    drain(hid_mid.at[:, pl.ds(1, outer - 1)], r.hid_ssem.at[0])
+    drain(hid_all.at[:, 0, pl.ds(1, inner - 1)], r.hid_ssem.at[2])
+
+    flat = r.up_send.at[0]
+    down = jnp.zeros((R, F), F32)
+    for c in range(chunks):
+        drain(flat.at[pl.ds(0, kv - 1)], r.hid_rsem.at[c])
+        for mz in range(outer):
+            group = flip(split(up_way[c])[0], mz)
+            begin = pl.multiple_of((c % parts) * span + group * (inner * CW), inner * CW)
+            down = down + jnp.dot(
+                jnp.concatenate([hid_all[c, mz, pt] for pt in range(inner)], axis=1),
+                r.v_w_down[c // parts, pl.ds(begin, inner * CW), :],
+                preferred_element_type=F32,
+            )
+    r.out[...] = (r.res_rows[...] + down * (factor_mid * factor_mid)).astype(BF16)
+    drain(hid_all.at[:, pl.ds(1, outer - 1)], r.hid_ssem.at[1])
+
+
+def named(
+    tokens,
+    gain_mix,
+    w_query,
+    w_key,
+    w_value,
+    w_igate,
+    w_fgate,
+    bias_igate,
+    bias_fgate,
+    state_mem,
+    state_max,
+    keys_blk,
+    values_blk,
+    igate_blk,
+    fgate_blk,
+    lengths,
+    gain_head,
+    w_mixout,
+    gain_mlp,
+    w_up,
+    w_down,
+):
+    return SimpleNamespace(**locals())
+
+
+def body(kv, tp, *args):
+    a = named(*args)
+    a.gain_mix, a.gain_head, a.gain_mlp, a.bias_igate, a.bias_fgate, a.lengths = (
+        x.reshape(1, -1)
+        for x in (a.gain_mix, a.gain_head, a.gain_mlp, a.bias_igate, a.bias_fgate, a.lengths)
+    )
+    a.w_igate, a.w_fgate = a.w_igate.T, a.w_fgate.T
+    rows, feats = a.tokens.shape
+    S, H, HD, _ = a.state_mem.shape
+    B = a.keys_blk.shape[2]
+    width = H * HD
+    inner = inner_size(kv)
+    outer = kv // inner
+    per = kv // tp
+    hidden = a.w_up.shape[1]
+    chunks = tp * max(n for n in (1, 2) if hidden % (n * kv * 128) == 0)
+    cw = hidden * tp // (chunks * kv)
+    V = pltpu.VMEM
+    dma = pltpu.SemaphoreType.DMA
+
+    def room(x, *many):
+        return V((*many, *x.shape), x.dtype)
+
+    scratch = dict(
+        v_tokens=room(a.tokens),
+        v_gain_mix=room(a.gain_mix),
+        v_lengths=room(a.lengths),
+        v_state_max=room(a.state_max),
+        v_gain_head=room(a.gain_head),
+        v_gain_mlp=room(a.gain_mlp),
+        v_state_mem=room(a.state_mem),
+        v_w_gate=room(a.w_igate, 2),
+        v_w_qkv=room(a.w_query, 3),
+        v_gate_blk=room(a.fgate_blk, 2),
+        v_bias=room(a.bias_igate, 2),
+        v_kv_blk=room(a.keys_blk, 2),
+        v_w_mixout=room(a.w_mixout, tp),
+        v_w_up=room(a.w_up, tp),
+        v_w_down=room(a.w_down, tp),
+        state_t=V(a.state_mem.shape, BF16),
+        keys_t=V((S, H, HD, B), BF16),
+        tok_peer=room(a.tokens),
+        proj_send=V((3, kv, S, width), BF16),
+        proj_recv=V((3, outer, inner, S, width), BF16),
+        proj_mid=V((3, outer, S, width), BF16),
+        proj_last=V((3, outer, S, width), BF16),
+        gate_send=V((kv, S, 128), F32),
+        gate_recv=V((kv, S, 128), F32),
+        mixed_own=V((S, width), BF16),
+        mixed_all=V((tp * per, S, width), BF16),
+        mixed_rows=V((rows, tp * width), F32),
+        res_rows=V((rows, feats), F32),
+        sq_all=V((kv, 1, 128), F32),
+        up_send=V((chunks, kv, rows, cw), BF16),
+        up_recv=V((chunks, outer, inner, rows, cw), BF16),
+        up_mid=V((chunks, outer, rows, cw), BF16),
+        up_last=V((chunks, outer, rows, cw), BF16),
+        hid_mid=V((chunks, outer, rows, cw), BF16),
+        hid_all=V((chunks, outer, inner, rows, cw), BF16),
+        local_sem=dma((15,)),
+        pair_ssem=dma((4,)),
+        pair_rsem=dma((4,)),
+        proj_ssem=dma,
+        proj_rsem=dma((3, 2)),
+        mid_ssem=dma((2,)),
+        mid_rsem=dma((3,)),
+        gate_ssem=dma,
+        gate_rsem=dma,
+        mix_ssem=dma,
+        mix_rsem=dma,
+        sq_ssem=dma,
+        sq_rsem=dma,
+        up_ssem=dma,
+        up_rsem=dma((chunks, 2)),
+        up_lsem=dma((chunks,)),
+        hid_ssem=dma((3,)),
+        hid_msem=dma((chunks, outer - 1)),
+        hid_rsem=dma((chunks,)),
+    )
+    operands = vars(a)
+    names = (*operands, "out", *scratch)
+    return pl.pallas_call(
+        functools.partial(kernel, (kv, tp, kv * feats), names),
+        out_shape=V((rows, feats), BF16),
+        in_specs=[pl.BlockSpec(memory_space=pl.ANY)] * len(operands),
+        out_specs=pl.BlockSpec(memory_space=V),
+        scratch_shapes=list(scratch.values()),
+        compiler_params=pltpu.CompilerParams(
+            collective_id=0, has_side_effects=True, vmem_limit_bytes=56 * 1024 * 1024
+        ),
+    )(*operands.values())
+
+
+def suits(kv, tp, *args):
+    a = named(*args)
+    inner = inner_size(kv)
+    outer = kv // inner
+    return (
+        tp == 2
+        and kv & (kv - 1) == 0
+        and outer > 1
+        and inner > 1
+        and a.tokens.shape[1] % 128 == 0
+        and a.tokens.shape[0] <= 128
+        and a.w_up.shape[1] % (kv * 128) == 0
+    )
+
+
+def either(kv, tp, *args):
+    return (body if suits(kv, tp, *args) else any_body)(kv, tp, *args)
+
+
 def solution(mesh):
     in_specs = (
         P("tp", "kv"),
@@ -660,5 +1353,5 @@
         P("tp", "kv"),
     )
     out_specs = P("tp", "kv")
-    run = functools.partial(body, mesh.shape["kv"], mesh.shape["tp"])
+    run = functools.partial(either, mesh.shape["kv"], mesh.shape["tp"])
     return jax.shard_map(run, mesh=mesh, in_specs=in_specs, out_specs=out_specs, check_vma=False)

time: 53.3 us -> 37.8 us (0.71)
  Pallas kernels: 48.9 us -> 37 us
  local copies, waits for them, and re-layouts: 4.08 us -> 0.6 us
    pallas_call x1, Pallas kernels: 48.9 us -> 37 us  [body(): pl.pallas_call(functools.partial(kernel, (kv, tp, kv * feats), names), ou...]
    unnamed x3 -> x1, local copies, waits for them, and re-layouts: 4.08 us -> 0.6 us
where the time goes in v1:
time: 37.8 us; the launch traced here: 37.6 us
  Pallas kernels  37 us (98%)
  local copies, waits for them, and re-layouts  0.6 us (2%)
    pallas_call x1, Pallas kernels, body(): pl.pallas_call(functools.partial(kernel, (kv, tp, kv * feats), names), ou...  37 us

profile of v1, /device:TPU:0, one launch (start us, length us, event | category | flops | bytes accessed | tf_op | source)
XLA Modules:
  0.0 37.6 jit_solution(12358425395467527009)
XLA Ops:
  0.0 37.0 %shard_map.199 = bf16[32,128]{1,0:T(8,128)(2,1)S(1)} custom-call(bf16[32,128]{1,0:T(8,128)(2,1)} %refs_0_.1, f32[1,128]{1,0:T(1,128)} %bitcast.11, bf16[128,1024]{1,0:T(8,128)(2,1)} %refs_2_.1, bf16[128,1024]{1,0:T(8,128)(2,1)} %refs_3_.1, bf16[128,1024]{1,0:T(8,128)(2,1)} %refs_4_.1, bf16[4,128]{1,0:T(4,128)(2,1)} %bitcast.8, bf16[4,128]{1,0:T(4,128)(2,1)} %bitcast.9, ...), custom_call_target="tpu_custom_call" | custom-call | tf_op jit(solution)/shard_map/pallas_call | solution.py:1300
  37.0 0.6 %copy.23 = bf16[32,128]{1,0:T(8,128)(2,1)} copy(bf16[32,128]{1,0:T(8,128)(2,1)S(1)} %shard_map.199) | data formatting | bytes 16384

commit v2 on v1

--- a/solution.py
+++ b/solution.py
@@ -681,19 +681,23 @@
     half = lax.div(me, per)
     jj_me = lax.rem(me, per)
     chunks, _, _, CW = r.up_send.shape
-    proj_way = [ways[a % len(ways)] for a in range(3)]
+    proj_way = [ways[a % len(ways)] for a in range(4)]
     up_way = [ways[c % len(ways)] for c in range(chunks)]
 
+    cube = kv // 2
     barrier = pltpu.get_barrier_semaphore()
 
     def greet(target, c):
         pl.semaphore_signal(barrier, inc=1, device_id=(target, c), device_id_type=MESH)
 
-    for m in reversed(range(1, kv)):
-        target = flip(me, m)
-        greet(target, core)
-        greet(target, other)
+    for m in reversed(range(1, cube)):
+        greet(flip(me, m), 1)
     greet(me, other)
+
+    @pl.when(core == 1)
+    def _():
+        greet(flip(me, cube), 1)
+
 
     taken = iter(range(r.local_sem.shape[0]))
 
@@ -741,7 +745,17 @@
     def drain(ref, sem):
         remote(ref, ref, sem, sem, me, other).wait_send()
 
-    loaded([got_tokens, got_gain_mix, got_w_gate])
+    tok_copy = remote(
+        r.v_tokens, r.tok_peer, r.pair_ssem.at[0], r.pair_rsem.at[0], me, other
+    )
+    got_tokens.wait()
+
+    @pl.when(core == 0)
+    def _():
+        pl.semaphore_wait(barrier, 1)
+        tok_copy.start()
+
+    loaded([got_gain_mix, got_w_gate])
     lane = lax.broadcasted_iota(jnp.int32, (H, 128), 1)
     sub = lax.broadcasted_iota(jnp.int32, (H, 128), 0)
     pick_i = (lane == sub).astype(F32).astype(BF16)
@@ -754,7 +768,11 @@
     lane_r = lax.broadcasted_iota(jnp.int32, (R, 128), 1)
     gain_mix = r.v_gain_mix[...]
     gate_send = r.gate_send
-    proj_send, proj_recv, proj_mid, proj_last = r.proj_send, r.proj_recv, r.proj_mid, r.proj_last
+    proj_send = r.proj_send
+    send_of = [*(proj_send.at[a] for a in range(3)), gate_send]
+    recv_of = [*(r.proj_recv.at[a] for a in range(3)), r.gate_recv]
+    mid_of = [*(r.proj_mid.at[a] for a in range(3)), r.gate_mid]
+    last_of = [*(r.proj_last.at[a] for a in range(3)), r.gate_last]
 
     def project(rows, group):
         scaled = (rows * gain_mix).astype(BF16)
@@ -791,12 +809,26 @@
         past = jnp.where(live, r.v_gate_blk[1, :, h, :] + suffix, -jnp.inf)
         carried = r.v_state_max[:, h : h + 1] + jnp.sum(forget, axis=1, keepdims=True)
         base.append((past, jnp.max(past, axis=1, keepdims=True), carried))
-    pl.semaphore_wait(barrier, kv * tp - 1)
-
-    tok_copy = remote(
-        r.v_tokens, r.tok_peer, r.pair_ssem.at[0], r.pair_rsem.at[0], me, other
-    )
-    tok_copy.start()
+    tok_copy.wait_recv()
+
+    @pl.when(core == 1)
+    def _():
+        tok_copy.start()
+
+    project(r.tok_peer[...].astype(F32), other)
+
+    @pl.when(core == 1)
+    def _():
+        pl.semaphore_wait(barrier, 2 * cube)
+        pl.semaphore_signal(r.go_sem, inc=1, device_id=(me, other), device_id_type=MESH)
+        pl.semaphore_signal(
+            r.half_sem, inc=1, device_id=(flip(me, cube), core), device_id_type=MESH
+        )
+
+    @pl.when(core == 0)
+    def _():
+        pl.semaphore_wait(r.go_sem, 1)
+
 
     def pair(i, ref):
         return remote(ref.at[0], ref.at[1], r.pair_ssem.at[i], r.pair_rsem.at[i], me, other)
@@ -806,9 +838,9 @@
     def proj_one(a, mz, mp):
         first, second = proj_way[a]
         return remote(
-            proj_send.at[a, flip(me, first[mp] + second[mz])],
-            proj_recv.at[a, mz, mp],
-            r.proj_ssem,
+            send_of[a].at[flip(me, first[mp] + second[mz])],
+            recv_of[a].at[mz, mp],
+            r.proj_ssem.at[a],
             r.proj_rsem.at[a, mz // (outer // 2)],
             flip(me, first[mp]),
             other,
@@ -816,9 +848,9 @@
 
     def proj_two(a, mz):
         return remote(
-            proj_mid.at[a, mz],
-            proj_last.at[a, mz],
-            r.mid_ssem.at[0],
+            mid_of[a].at[mz],
+            last_of[a].at[mz],
+            r.mid_ssem.at[a],
             r.mid_rsem.at[a],
             flip(me, proj_way[a][1][mz]),
             other,
@@ -833,46 +865,8 @@
             for mp in peers:
                 proj_one(a, mz, mp).start()
 
-    def gate_copy(m):
-        return remote(
-            gate_send.at[flip(me, m)],
-            r.gate_recv.at[m],
-            r.gate_ssem,
-            r.gate_rsem,
-            flip(me, m),
-            core,
-        )
-
-    far_m = [m for m in reversed(range(1, kv)) if m >= per]
-    near_m = [m for m in reversed(range(1, kv)) if m < per]
-
-    @pl.when(core != half)
-    def _():
-        for m in far_m:
-            gate_copy(m).start()
-        for a in range(3):
-            send_groups(a, far)
-
-    tok_copy.wait_recv()
-    peer_rows = r.tok_peer[...].astype(F32)
-    project(peer_rows, other)
-
-    @pl.when(core == half)
-    def _():
-        for m in far_m:
-            gate_copy(m).start()
-        send_groups(0, far)
-
-    for m in near_m:
-        gate_copy(m).start()
-    send_groups(0, near)
-
-    @pl.when(core == half)
-    def _():
-        for a in (1, 2):
-            send_groups(a, far)
-
-    for a in (1, 2):
+    for a in (3, 0, 1, 2):
+        send_groups(a, far)
         send_groups(a, near)
 
     got_w_mixout.wait()
@@ -897,40 +891,48 @@
     def proj_middle(a):
         for side, groups in ((1, far), (0, near)):
             drain(
-                proj_recv.at[a, pl.ds(side * (outer // 2), outer // 2)], r.proj_rsem.at[a, side]
+                recv_of[a].at[pl.ds(side * (outer // 2), outer // 2)], r.proj_rsem.at[a, side]
             )
             for mz in groups:
-                proj_mid[a, mz] = summed(proj_recv.at[a, mz]).astype(BF16)
+                mid_of[a][mz] = summed(recv_of[a].at[mz]).astype(mid_of[a].dtype)
                 proj_two(a, mz).start()
 
     def proj_end(a):
-        drain(proj_last.at[a], r.mid_rsem.at[a])
-        return (summed(proj_last.at[a]) * factor_in).astype(BF16)
-
-    proj_middle(0)
-    proj_middle(1)
-    proj_middle(2)
+        drain(last_of[a], r.mid_rsem.at[a])
+        return summed(last_of[a])
+
+    @pl.when(core == 1)
+    def _():
+        pl.semaphore_wait(r.half_sem, 1)
+        pl.semaphore_signal(r.half_sem, inc=1, device_id=(me, other), device_id_type=MESH)
+
+    @pl.when(core == 0)
+    def _():
+        pl.semaphore_wait(r.half_sem, 1)
+
+    for a in (3, 0, 1, 2):
+        proj_middle(a)
     got_w_up.wait()
     pairs[1].start()
-    drain(r.gate_recv.at[pl.ds(1, kv - 1)], r.gate_rsem)
-    gate_sum = gate_send[me]
-    for m in range(1, kv):
-        gate_sum = gate_sum + r.gate_recv[m]
+    gate_sum = proj_end(3)
     factor_in = lax.rsqrt(gate_sum[:, 2 * H : 2 * H + 1] / D + EPS)
     gate_sum = gate_sum * factor_in
-    query = proj_end(0)
-
     scale = HD ** (-0.5)
-    cells = []
+    shares = []
     for h in range(H):
-        q = query[:, h * HD : (h + 1) * HD]
         past, past_top, carried = base[h]
         ig = gate_sum[:, h : h + 1] + r.v_bias[0, :, h : h + 1]
         raw = gate_sum[:, H + h : H + h + 1] + r.v_bias[1, :, h : h + 1]
         fg = jnp.minimum(raw, 0.0) - jnp.log1p(jnp.exp(-jnp.abs(raw)))
         carried = carried + fg
         top = jnp.maximum(jnp.maximum(carried, ig), past_top + fg)
-        decay = jnp.exp(past + (fg - top))
+        shares.append((jnp.exp(past + (fg - top)) * scale, jnp.exp(carried - top), jnp.exp(ig - top)))
+    query = (proj_end(0) * factor_in).astype(BF16)
+
+    cells = []
+    for h in range(H):
+        q = query[:, h * HD : (h + 1) * HD]
+        decay, remaining, entering = shares[h]
         scores = jnp.zeros((S, B), F32)
         state_term = jnp.zeros((S, HD), F32)
         for s in range(S):
@@ -939,15 +941,15 @@
             scores = jnp.where(mine, got, scores)
             mem = jnp.dot(q, r.state_t[s, h], preferred_element_type=F32)
             state_term = jnp.where(mine, mem, state_term)
-        weights = (decay * (scores * scale)).astype(BF16)
+        weights = (decay * scores).astype(BF16)
         block_term = jnp.zeros((S, HD), F32)
         for s in range(S):
             got = jnp.dot(weights, r.v_kv_blk[1, s, h], preferred_element_type=F32)
             block_term = jnp.where(row == s, got, block_term)
-        cells.append((state_term * jnp.exp(carried - top) + block_term, jnp.exp(ig - top)))
-
-    key_new = proj_end(1)
-    value_new = proj_end(2)
+        cells.append((state_term * remaining + block_term, entering))
+
+    key_new = (proj_end(1) * factor_in).astype(BF16)
+    value_new = (proj_end(2) * factor_in).astype(BF16)
     for h in range(H):
         cols = slice(h * HD, (h + 1) * HD)
         q, k, v = query[:, cols], key_new[:, cols], value_new[:, cols]
@@ -1029,7 +1031,7 @@
         return remote(
             up_mid.at[c, mz],
             up_last.at[c, mz],
-            r.mid_ssem.at[1],
+            r.mid_ssem.at[4],
             r.up_lsem.at[c],
             flip(me, up_way[c][1][mz]),
             other,
@@ -1149,9 +1151,9 @@
         step(*which)
 
     tok_copy.wait_send()
-    drain(r.gate_recv.at[pl.ds(1, kv - 1)], r.gate_ssem)
-    drain(proj_recv, r.proj_ssem)
-    drain(proj_last, r.mid_ssem.at[0])
+    for a in range(4):
+        drain(recv_of[a], r.proj_ssem.at[a])
+        drain(last_of[a], r.mid_ssem.at[a])
 
     @pl.when(slot == 0)
     def _():
@@ -1163,7 +1165,7 @@
 
     drain(r.sq_all.at[pl.ds(1, kv - 1)], r.sq_ssem)
     drain(up_recv, r.up_ssem)
-    drain(up_last, r.mid_ssem.at[1])
+    drain(up_last, r.mid_ssem.at[4])
     pairs[2].wait()
     drain(r.sq_all.at[pl.ds(1, kv - 1)], r.sq_rsem)
     squares = r.sq_all[0]
@@ -1263,7 +1265,9 @@
         proj_mid=V((3, outer, S, width), BF16),
         proj_last=V((3, outer, S, width), BF16),
         gate_send=V((kv, S, 128), F32),
-        gate_recv=V((kv, S, 128), F32),
+        gate_recv=V((outer, inner, S, 128), F32),
+        gate_mid=V((outer, S, 128), F32),
+        gate_last=V((outer, S, 128), F32),
         mixed_own=V((S, width), BF16),
         mixed_all=V((tp * per, S, width), BF16),
         mixed_rows=V((rows, tp * width), F32),
@@ -1278,12 +1282,10 @@
         local_sem=dma((15,)),
         pair_ssem=dma((4,)),
         pair_rsem=dma((4,)),
-        proj_ssem=dma,
-        proj_rsem=dma((3, 2)),
-        mid_ssem=dma((2,)),
-        mid_rsem=dma((3,)),
-        gate_ssem=dma,
-        gate_rsem=dma,
+        proj_ssem=dma((4,)),
+        proj_rsem=dma((4, 2)),
+        mid_ssem=dma((5,)),
+        mid_rsem=dma((4,)),
         mix_ssem=dma,
         mix_rsem=dma,
         sq_ssem=dma,
@@ -1294,6 +1296,8 @@
         hid_ssem=dma((3,)),
         hid_msem=dma((chunks, outer - 1)),
         hid_rsem=dma((chunks,)),
+        go_sem=pltpu.SemaphoreType.REGULAR,
+        half_sem=pltpu.SemaphoreType.REGULAR,
     )
     operands = vars(a)
     names = (*operands, "out", *scratch)

time: 37.8 us -> 36.6 us (0.968)
  Pallas kernels: 37 us -> 35.8 us
    pallas_call x1, Pallas kernels: 37 us -> 35.8 us  [body(): pl.pallas_call(functools.partial(kernel, (kv, tp, kv * feats), names), ou...]
where the time goes in v2:
time: 36.6 us; the launch traced here: 36.4 us
  Pallas kernels  35.8 us (98%)
  local copies, waits for them, and re-layouts  0.6 us (2%)
    pallas_call x1, Pallas kernels, body(): pl.pallas_call(functools.partial(kernel, (kv, tp, kv * feats), names), ou...  35.8 us

profile of v2, /device:TPU:0, one launch (start us, length us, event | category | flops | bytes accessed | tf_op | source)
XLA Modules:
  0.0 36.4 jit_solution(2539445900874314746)
XLA Ops:
  0.0 35.8 %shard_map.199 = bf16[32,128]{1,0:T(8,128)(2,1)S(1)} custom-call(bf16[32,128]{1,0:T(8,128)(2,1)} %refs_0_.1, f32[1,128]{1,0:T(1,128)} %bitcast.11, bf16[128,1024]{1,0:T(8,128)(2,1)} %refs_2_.1, bf16[128,1024]{1,0:T(8,128)(2,1)} %refs_3_.1, bf16[128,1024]{1,0:T(8,128)(2,1)} %refs_4_.1, bf16[4,128]{1,0:T(4,128)(2,1)} %bitcast.8, bf16[4,128]{1,0:T(4,128)(2,1)} %bitcast.9, ...), custom_call_target="tpu_custom_call" | custom-call | tf_op jit(solution)/shard_map/pallas_call | solution.py:1304
  35.8 0.6 %copy.23 = bf16[32,128]{1,0:T(8,128)(2,1)} copy(bf16[32,128]{1,0:T(8,128)(2,1)S(1)} %shard_map.199) | data formatting | bytes 16384

commit v3 on v2

--- a/solution.py
+++ b/solution.py
@@ -685,14 +685,17 @@
     up_way = [ways[c % len(ways)] for c in range(chunks)]
 
     cube = kv // 2
+    reach = {m for first, _ in ways for m in first if m}
+    reach |= {m % cube for _, second in ways for m in second if m % cube}
+
     barrier = pltpu.get_barrier_semaphore()
 
     def greet(target, c):
         pl.semaphore_signal(barrier, inc=1, device_id=(target, c), device_id_type=MESH)
 
-    for m in reversed(range(1, cube)):
+    greet(me, other)
+    for m in sorted(reach, reverse=True):
         greet(flip(me, m), 1)
-    greet(me, other)
 
     @pl.when(core == 1)
     def _():
@@ -724,9 +727,6 @@
         load(r.v_gain_head, r.gain_head),
     ]
     got_gain_mlp = load(r.v_gain_mlp, r.gain_mlp)
-    got_w_mixout = load(r.v_w_mixout.at[0], r.w_mixout)
-    got_w_up = load(r.v_w_up.at[0], r.w_up)
-    got_w_down = load(r.v_w_down.at[0], r.w_down)
 
     def loaded(copies):
         for copy in copies:
@@ -748,12 +748,18 @@
     tok_copy = remote(
         r.v_tokens, r.tok_peer, r.pair_ssem.at[0], r.pair_rsem.at[0], me, other
     )
-    got_tokens.wait()
 
     @pl.when(core == 0)
     def _():
         pl.semaphore_wait(barrier, 1)
-        tok_copy.start()
+        pl.semaphore_signal(r.hello_sem, inc=1, device_id=(me, other), device_id_type=MESH)
+
+    @pl.when(core == 1)
+    def _():
+        pl.semaphore_wait(r.hello_sem, 1)
+
+    got_tokens.wait()
+    tok_copy.start()
 
     loaded([got_gain_mix, got_w_gate])
     lane = lax.broadcasted_iota(jnp.int32, (H, 128), 1)
@@ -790,6 +796,110 @@
     got_w_qkv.wait()
     project(own_rows, core)
 
+    tok_copy.wait_recv()
+    project(r.tok_peer[...].astype(F32), other)
+
+    @pl.when(core == 1)
+    def _():
+        pl.semaphore_wait(barrier, 2 * len(reach) + 2)
+        pl.semaphore_signal(r.go_sem, inc=1, device_id=(me, other), device_id_type=MESH)
+        pl.semaphore_signal(
+            r.half_sem, inc=1, device_id=(flip(me, cube), core), device_id_type=MESH
+        )
+
+    @pl.when(core == 0)
+    def _():
+        pl.semaphore_wait(r.go_sem, 1)
+
+
+    def pair(i, ref):
+        return remote(ref.at[0], ref.at[1], r.pair_ssem.at[i], r.pair_rsem.at[i], me, other)
+
+    pairs = [pair(1, r.v_w_mixout), pair(2, r.v_w_up), pair(3, r.v_w_down)]
+
+    def proj_one(a, mz, mp):
+        first, second = proj_way[a]
+        return remote(
+            send_of[a].at[flip(me, first[mp] + second[mz])],
+            recv_of[a].at[mz, mp],
+            r.proj_ssem.at[a],
+            r.proj_rsem.at[a, mz // (outer // 2)],
+            flip(me, first[mp]),
+            other,
+        )
+
+    def proj_two(a, mz):
+        return remote(
+            mid_of[a].at[mz],
+            last_of[a].at[mz],
+            r.mid_ssem.at[a],
+            r.mid_rsem.at[a],
+            flip(me, proj_way[a][1][mz]),
+            other,
+        )
+
+    far = [mz for mz in reversed(range(outer)) if mz >= outer // 2]
+    near = [mz for mz in reversed(range(outer)) if mz < outer // 2]
+    peers = list(reversed(range(inner)))
+
+    def send_groups(a, groups):
+        for mz in groups:
+            for mp in peers:
+                proj_one(a, mz, mp).start()
+
+    for a in (3, 0, 1, 2):
+        send_groups(a, far)
+        send_groups(a, near)
+
+    got_w_mixout = load(r.v_w_mixout.at[0], r.w_mixout)
+    got_w_up = load(r.v_w_up.at[0], r.w_up)
+    got_w_down = load(r.v_w_down.at[0], r.w_down)
+
+    loaded(got_memory)
+
+    def narrow(i, carry):
+        s, h = lax.div(i, H), lax.rem(i, H)
+        r.state_t[s, h] = r.v_state_mem[s, h].T.astype(BF16)
+        r.keys_t[s, h] = r.v_kv_blk[0, s, h].T
+        return carry
+
+    lax.fori_loop(0, S * H, narrow, 0)
+    got_w_mixout.wait()
+    pairs[0].start()
+
+    def summed(ref):
+        total = ref[0].astype(F32)
+        for i in range(1, ref.shape[0]):
+            total = total + ref[i].astype(F32)
+        return total
+
+    def proj_middle(a):
+        for side, groups in ((1, far), (0, near)):
+            drain(
+                recv_of[a].at[pl.ds(side * (outer // 2), outer // 2)], r.proj_rsem.at[a, side]
+            )
+            for mz in groups:
+                mid_of[a][mz] = summed(recv_of[a].at[mz]).astype(mid_of[a].dtype)
+                proj_two(a, mz).start()
+
+    def proj_end(a):
+        drain(last_of[a], r.mid_rsem.at[a])
+        return summed(last_of[a])
+
+    @pl.when(core == 1)
+    def _():
+        pl.semaphore_wait(r.half_sem, 1)
+        pl.semaphore_signal(r.half_sem, inc=1, device_id=(me, other), device_id_type=MESH)
+
+    @pl.when(core == 0)
+    def _():
+        pl.semaphore_wait(r.half_sem, 1)
+
+    for a in (3, 0, 1, 2):
+        proj_middle(a)
+    got_w_up.wait()
+    pairs[1].start()
+
     loaded(got_blk)
     row = lax.broadcasted_iota(jnp.int32, (S, 1), 0)
     eye_s = lax.broadcasted_iota(jnp.int32, (S, S), 0) == lax.broadcasted_iota(jnp.int32, (S, S), 1)
@@ -809,111 +919,6 @@
         past = jnp.where(live, r.v_gate_blk[1, :, h, :] + suffix, -jnp.inf)
         carried = r.v_state_max[:, h : h + 1] + jnp.sum(forget, axis=1, keepdims=True)
         base.append((past, jnp.max(past, axis=1, keepdims=True), carried))
-    tok_copy.wait_recv()
-
-    @pl.when(core == 1)
-    def _():
-        tok_copy.start()
-
-    project(r.tok_peer[...].astype(F32), other)
-
-    @pl.when(core == 1)
-    def _():
-        pl.semaphore_wait(barrier, 2 * cube)
-        pl.semaphore_signal(r.go_sem, inc=1, device_id=(me, other), device_id_type=MESH)
-        pl.semaphore_signal(
-            r.half_sem, inc=1, device_id=(flip(me, cube), core), device_id_type=MESH
-        )
-
-    @pl.when(core == 0)
-    def _():
-        pl.semaphore_wait(r.go_sem, 1)
-
-
-    def pair(i, ref):
-        return remote(ref.at[0], ref.at[1], r.pair_ssem.at[i], r.pair_rsem.at[i], me, other)
-
-    pairs = [pair(1, r.v_w_mixout), pair(2, r.v_w_up), pair(3, r.v_w_down)]
-
-    def proj_one(a, mz, mp):
-        first, second = proj_way[a]
-        return remote(
-            send_of[a].at[flip(me, first[mp] + second[mz])],
-            recv_of[a].at[mz, mp],
-            r.proj_ssem.at[a],
-            r.proj_rsem.at[a, mz // (outer // 2)],
-            flip(me, first[mp]),
-            other,
-        )
-
-    def proj_two(a, mz):
-        return remote(
-            mid_of[a].at[mz],
-            last_of[a].at[mz],
-            r.mid_ssem.at[a],
-            r.mid_rsem.at[a],
-            flip(me, proj_way[a][1][mz]),
-            other,
-        )
-
-    far = [mz for mz in reversed(range(outer)) if mz >= outer // 2]
-    near = [mz for mz in reversed(range(outer)) if mz < outer // 2]
-    peers = list(reversed(range(inner)))
-
-    def send_groups(a, groups):
-        for mz in groups:
-            for mp in peers:
-                proj_one(a, mz, mp).start()
-
-    for a in (3, 0, 1, 2):
-        send_groups(a, far)
-        send_groups(a, near)
-
-    got_w_mixout.wait()
-    pairs[0].start()
-
-    loaded(got_memory)
-
-    def narrow(i, carry):
-        s, h = lax.div(i, H), lax.rem(i, H)
-        r.state_t[s, h] = r.v_state_mem[s, h].T.astype(BF16)
-        r.keys_t[s, h] = r.v_kv_blk[0, s, h].T
-        return carry
-
-    lax.fori_loop(0, S * H, narrow, 0)
-
-    def summed(ref):
-        total = ref[0].astype(F32)
-        for i in range(1, ref.shape[0]):
-            total = total + ref[i].astype(F32)
-        return total
-
-    def proj_middle(a):
-        for side, groups in ((1, far), (0, near)):
-            drain(
-                recv_of[a].at[pl.ds(side * (outer // 2), outer // 2)], r.proj_rsem.at[a, side]
-            )
-            for mz in groups:
-                mid_of[a][mz] = summed(recv_of[a].at[mz]).astype(mid_of[a].dtype)
-                proj_two(a, mz).start()
-
-    def proj_end(a):
-        drain(last_of[a], r.mid_rsem.at[a])
-        return summed(last_of[a])
-
-    @pl.when(core == 1)
-    def _():
-        pl.semaphore_wait(r.half_sem, 1)
-        pl.semaphore_signal(r.half_sem, inc=1, device_id=(me, other), device_id_type=MESH)
-
-    @pl.when(core == 0)
-    def _():
-        pl.semaphore_wait(r.half_sem, 1)
-
-    for a in (3, 0, 1, 2):
-        proj_middle(a)
-    got_w_up.wait()
-    pairs[1].start()
     gate_sum = proj_end(3)
     factor_in = lax.rsqrt(gate_sum[:, 2 * H : 2 * H + 1] / D + EPS)
     gate_sum = gate_sum * factor_in
@@ -929,19 +934,24 @@
         shares.append((jnp.exp(past + (fg - top)) * scale, jnp.exp(carried - top), jnp.exp(ig - top)))
     query = (proj_end(0) * factor_in).astype(BF16)
 
-    cells = []
+    cells, weights_of, state_of = [], [], []
     for h in range(H):
         q = query[:, h * HD : (h + 1) * HD]
-        decay, remaining, entering = shares[h]
         scores = jnp.zeros((S, B), F32)
+        for s in range(S):
+            got = jnp.dot(q, r.keys_t[s, h], preferred_element_type=F32)
+            scores = jnp.where(row == s, got, scores)
+        weights_of.append((shares[h][0] * scores).astype(BF16))
+    for h in range(H):
+        q = query[:, h * HD : (h + 1) * HD]
         state_term = jnp.zeros((S, HD), F32)
         for s in range(S):
-            mine = row == s
-            got = jnp.dot(q, r.keys_t[s, h], preferred_element_type=F32)
-            scores = jnp.where(mine, got, scores)
             mem = jnp.dot(q, r.state_t[s, h], preferred_element_type=F32)
-            state_term = jnp.where(mine, mem, state_term)
-        weights = (decay * scores).astype(BF16)
+            state_term = jnp.where(row == s, mem, state_term)
+        state_of.append(state_term)
+    for h in range(H):
+        weights, state_term = weights_of[h], state_of[h]
+        _, remaining, entering = shares[h]
         block_term = jnp.zeros((S, HD), F32)
         for s in range(S):
             got = jnp.dot(weights, r.v_kv_blk[1, s, h], preferred_element_type=F32)
@@ -1298,6 +1308,7 @@
         hid_rsem=dma((chunks,)),
         go_sem=pltpu.SemaphoreType.REGULAR,
         half_sem=pltpu.SemaphoreType.REGULAR,
+        hello_sem=pltpu.SemaphoreType.REGULAR,
     )
     operands = vars(a)
     names = (*operands, "out", *scratch)

time: 36.6 us -> 36.3 us (level)
  no operation moved by 1% of the time
where the time goes in v3:
time: 36.3 us; the launch traced here: 36.2 us
  Pallas kernels  35.5 us (98%)
  local copies, waits for them, and re-layouts  0.6 us (2%)
    pallas_call x1, Pallas kernels, body(): pl.pallas_call(functools.partial(kernel, (kv, tp, kv * feats), names), ou...  35.5 us

profile of v3, /device:TPU:0, one launch (start us, length us, event | category | flops | bytes accessed | tf_op | source)
XLA Modules:
  0.0 36.2 jit_solution(10119838942286519089)
XLA Ops:
  0.0 35.5 %shard_map.199 = bf16[32,128]{1,0:T(8,128)(2,1)S(1)} custom-call(bf16[32,128]{1,0:T(8,128)(2,1)} %refs_0_.1, f32[1,128]{1,0:T(1,128)} %bitcast.11, bf16[128,1024]{1,0:T(8,128)(2,1)} %refs_2_.1, bf16[128,1024]{1,0:T(8,128)(2,1)} %refs_3_.1, bf16[128,1024]{1,0:T(8,128)(2,1)} %refs_4_.1, bf16[4,128]{1,0:T(4,128)(2,1)} %bitcast.8, bf16[4,128]{1,0:T(4,128)(2,1)} %bitcast.9, ...), custom_call_target="tpu_custom_call" | custom-call | tf_op jit(solution)/shard_map/pallas_call | solution.py:1315
  35.6 0.6 %copy.23 = bf16[32,128]{1,0:T(8,128)(2,1)} copy(bf16[32,128]{1,0:T(8,128)(2,1)S(1)} %shard_map.199) | data formatting | bytes 16384

commit v4 on v3

--- a/solution.py
+++ b/solution.py
@@ -822,7 +822,7 @@
         return remote(
             send_of[a].at[flip(me, first[mp] + second[mz])],
             recv_of[a].at[mz, mp],
-            r.proj_ssem.at[a],
+            r.proj_ssem.at[a // 3],
             r.proj_rsem.at[a, mz // (outer // 2)],
             flip(me, first[mp]),
             other,
@@ -832,7 +832,7 @@
         return remote(
             mid_of[a].at[mz],
             last_of[a].at[mz],
-            r.mid_ssem.at[a],
+            r.mid_ssem.at[a // 3],
             r.mid_rsem.at[a],
             flip(me, proj_way[a][1][mz]),
             other,
@@ -1041,7 +1041,7 @@
         return remote(
             up_mid.at[c, mz],
             up_last.at[c, mz],
-            r.mid_ssem.at[4],
+            r.mid_ssem.at[2],
             r.up_lsem.at[c],
             flip(me, up_way[c][1][mz]),
             other,
@@ -1145,7 +1145,7 @@
             hid_two(c, mz, mp).start()
 
     def hops(mz):
-        return 1.8 + 0.7 * ((mz & 1) + 2 * (mz >> 1)) if mz else 0.9
+        return 2.2 + 0.5 * ((mz & 1) + 2 * (mz >> 1)) if mz else 0.9
 
     steps, ready = [], [0.0] * chunks
     for i, (c, side) in enumerate(plan):
@@ -1161,9 +1161,9 @@
         step(*which)
 
     tok_copy.wait_send()
-    for a in range(4):
-        drain(recv_of[a], r.proj_ssem.at[a])
-        drain(last_of[a], r.mid_ssem.at[a])
+    for i, (sent, then) in enumerate(((r.proj_recv, r.proj_last), (r.gate_recv, r.gate_last))):
+        drain(sent, r.proj_ssem.at[i])
+        drain(then, r.mid_ssem.at[i])
 
     @pl.when(slot == 0)
     def _():
@@ -1175,7 +1175,7 @@
 
     drain(r.sq_all.at[pl.ds(1, kv - 1)], r.sq_ssem)
     drain(up_recv, r.up_ssem)
-    drain(up_last, r.mid_ssem.at[4])
+    drain(up_last, r.mid_ssem.at[2])
     pairs[2].wait()
     drain(r.sq_all.at[pl.ds(1, kv - 1)], r.sq_rsem)
     squares = r.sq_all[0]
@@ -1292,9 +1292,9 @@
         local_sem=dma((15,)),
         pair_ssem=dma((4,)),
         pair_rsem=dma((4,)),
-        proj_ssem=dma((4,)),
+        proj_ssem=dma((2,)),
         proj_rsem=dma((4, 2)),
-        mid_ssem=dma((5,)),
+        mid_ssem=dma((3,)),
         mid_rsem=dma((4,)),
         mix_ssem=dma,
         mix_rsem=dma,

time: 36.3 us -> 36.3 us (level)
  no operation moved by 1% of the time
where the time goes in v4:
time: 36.3 us; the launch traced here: 36.1 us
  Pallas kernels  35.5 us (98%)
  local copies, waits for them, and re-layouts  0.6 us (2%)
    pallas_call x1, Pallas kernels, body(): pl.pallas_call(functools.partial(kernel, (kv, tp, kv * feats), names), ou...  35.5 us

profile of v4, /device:TPU:0, one launch (start us, length us, event | category | flops | bytes accessed | tf_op | source)
XLA Modules:
  0.0 36.1 jit_solution(13863976925799005149)
XLA Ops:
  0.0 35.5 %shard_map.199 = bf16[32,128]{1,0:T(8,128)(2,1)S(1)} custom-call(bf16[32,128]{1,0:T(8,128)(2,1)} %refs_0_.1, f32[1,128]{1,0:T(1,128)} %bitcast.11, bf16[128,1024]{1,0:T(8,128)(2,1)} %refs_2_.1, bf16[128,1024]{1,0:T(8,128)(2,1)} %refs_3_.1, bf16[128,1024]{1,0:T(8,128)(2,1)} %refs_4_.1, bf16[4,128]{1,0:T(4,128)(2,1)} %bitcast.8, bf16[4,128]{1,0:T(4,128)(2,1)} %bitcast.9, ...), custom_call_target="tpu_custom_call" | custom-call | tf_op jit(solution)/shard_map/pallas_call | solution.py:1315
  35.5 0.6 %copy.23 = bf16[32,128]{1,0:T(8,128)(2,1)} copy(bf16[32,128]{1,0:T(8,128)(2,1)S(1)} %shard_map.199) | data formatting | bytes 16384
